TPU v7x, 512 devices: a whole 4x8x8 slice. The times are simulated.
512 devices in a mesh: sp: 32 (over z, x), tp: 16 (over y, core).
Axes of the slice: x: 4, y: 8, z: 8, core: 2. Of those that a mesh axis runs over, the one named last changes fastest.
Arguments:
- resid: bfloat16 [16384, 2048], P(('sp', 'tp')), may hold values from -6 to 6
- recurrent_input: bfloat16 [16384, 2048], P('sp', 'tp'), may hold values from -12.2 to 12.2
- recurrent_out_gate: bfloat16 [16384, 2048], P('sp', 'tp'), may hold values from -6 to 6
- filter_weight: float32 [4, 2048], P(None, 'tp'), may hold values from -3 to 3
- recurrence_gate_matrix: bfloat16 [32, 64, 64], P('tp'), may hold values from -0.75 to 0.75
- input_gate_matrix: bfloat16 [32, 64, 64], P('tp'), may hold values from -0.75 to 0.75
- channel_decay_raw: float32 [2048], P('tp'), may hold values from 4.8 to 13.5
- token_decay_boost: float32 [16384, 2048], P('sp', 'tp'), may hold values from -0.7 to 0
- output_projection_weight: bfloat16 [2048, 2048], P('tp'), may hold values from -0.375 to 0.375
- expert_norm_gain: float32 [2048], replicated, may hold values from 0.1 to 1.9
- routes: int32 [16384, 2], P('sp'), may hold values from 0 to 31, all different within a row; in each aligned block of 32 rows (0 to 31, 32 to 63, ...) at most 3 rows name the same one
- expert_pair_weight: float32 [16384, 2], P(('sp', 'tp')), may hold values from 0.2 to 0.8
- gate_weight: bfloat16 [32, 2048, 2048], P('sp', None, 'tp'), may hold values from -0.125 to 0.125
- up_weight: bfloat16 [32, 2048, 2048], P('sp', None, 'tp'), may hold values from -0.125 to 0.125
- down_weight: bfloat16 [32, 2048, 2048], P('sp', None, 'tp'), may hold values from -0.25 to 0.25
Outputs:
- layer_out: bfloat16 [16384, 2048], P(('sp', 'tp'))
Inputs may be any that keep to these rules, and one draw needn't show every extreme that they name: `routes`: in each aligned block of 32 rows no expert is named by more than 3 rows, and the two experts of a row differ.
All inputs are finite; a program needn't handle non-finite values.
Results may differ from a plain program's by a relative error of at most 0.013.
Values may be sent and summed in bfloat16 or wider, within the bound.
No kernel may reach another device: no remote copies, remote signals or barrier semaphores. Data moves between devices by JAX's collectives and lax.ppermute only.
A program may use at most 64 MiB of HBM per device.

v0:
```python
import jax
import jax.numpy as jnp
from jax import lax
from jax.sharding import PartitionSpec as P

RECURRENT_SCALE = 8.0
EPSILON = 1e-06


def shifted(block, axis, distance):
    devices = range(lax.axis_size(axis))
    route = [(i - distance, i) for i in devices if i - distance in devices]
    return lax.ppermute(block, axis, route)


def from_everyone(x, axis):
    size = lax.axis_size(axis)
    return lax.all_to_all(jnp.broadcast_to(x[None], (size, *x.shape)), axis, 0, 0, tiled=True)


def collected_together(x, axis):
    leaves = jax.tree.leaves(x)
    order = sorted(range(len(leaves)), key=lambda k: -leaves[k].size)
    width = (1, *leaves[order[0]].shape)[-1]
    lines = [
        jnp.pad(leaves[k].reshape(-1), (0, -leaves[k].size % width)).reshape(-1, width)
        for k in order
    ]
    both, at, found = (from_everyone(jnp.concatenate(lines), axis), 0, {})
    for k, line in zip(order, lines):
        slab = both[:, at : at + len(line)].reshape(len(both), -1)
        found[k] = slab[:, : leaves[k].size].reshape(-1, *leaves[k].shape)
        at += len(line)
    numbers = iter(range(len(leaves)))
    return jax.tree.map(lambda _: found[next(numbers)], x)


def joined_by_halves(pieces, combine):
    while len(jax.tree.leaves(pieces)[0]) > 1:
        pieces = jax.vmap(combine)(
            *(jax.tree.map(lambda part: part[side::2], pieces) for side in (0, 1))
        )
    return jax.tree.map(lambda part: part[0], pieces)


def carried_in(x, axis, combine, identity):
    size, position = (lax.axis_size(axis), lax.axis_index(axis))
    passed = jnp.arange(size) < position

    def kept(part, zero, own):
        part = jnp.where(
            passed.reshape(-1, *(1 for _ in own.shape)), part, jnp.asarray(zero, own.dtype)
        )
        return part

    pieces = collected_together(x, axis)
    return joined_by_halves(jax.tree.map(kept, pieces, identity, x), combine)


def split_up(x, dim, size):
    before, after = (x.shape[:dim], x.shape[dim + 1 :])
    return jnp.moveaxis(x.reshape(*before, size, -1, *after), dim, 0)


def sum_at_owner(x, axis, dim):
    pieces = split_up(x, dim, lax.axis_size(axis))
    arrived = lax.all_to_all(pieces, axis, split_axis=0, concat_axis=0, tiled=True)
    return arrived.astype(jnp.float32).sum(axis=0)


def in_order(pieces, dim):
    pieces = jnp.moveaxis(pieces, 0, dim)
    dims = pieces.shape
    return pieces.reshape(*dims[:dim], dims[dim] * dims[dim + 1], *dims[dim + 2 :])


def piecewise(x, axis, dim, work, out_dim):
    extent = x.shape[dim]
    pieces = jnp.split(x, 2, axis=dim) if extent % 2 == 0 else [x]
    first = jnp.arange(lax.axis_size(axis)) * extent
    blocks = [lax.all_gather(slab, axis) for slab in pieces]
    made = [jax.vmap(work)(b, first + k * (extent // len(pieces))) for k, b in enumerate(blocks)]
    return in_order(jnp.concatenate(made, axis=out_dim + 1), out_dim)


def chain_step(earlier, later):
    return (earlier[0] * later[0], later[0] * earlier[1] + later[1])


def slot_numbers(picks, experts):
    flat = picks.reshape(-1)
    onehot = (flat[:, None] == jnp.arange(experts, dtype=jnp.int32)[None, :]).astype(jnp.int32)
    before = jnp.cumsum(onehot, axis=0) - onehot
    return (flat, jnp.sum(before * onehot, axis=1))


def fill_slots(source_rows, slot_of, row_of, slot_count):
    match = slot_of[None, :] == jnp.arange(slot_count, dtype=jnp.int32)[:, None]
    picked = jnp.sum(jnp.where(match, row_of[None, :], 0), axis=1)
    present = jnp.any(match, axis=1)
    return jnp.where(present[:, None], source_rows[picked], jnp.zeros((), source_rows.dtype))


def expert_hidden(rows, gate_weight, up_weight):
    gate = jnp.dot(rows, gate_weight[0], preferred_element_type=jnp.float32)
    upward = jnp.dot(rows, up_weight[0], preferred_element_type=jnp.float32)
    return (jax.nn.silu(gate) * upward).astype(jnp.bfloat16)


def expert_down(active, down_weight):
    columns = down_weight[0]
    return jnp.dot(
        lax.all_gather(active, "tp", axis=1, tiled=True),
        columns,
        preferred_element_type=jnp.float32,
    ).astype(jnp.bfloat16)


def body(
    resid,
    recurrent_input,
    recurrent_out_gate,
    filter_weight,
    recurrence_gate_matrix,
    input_gate_matrix,
    channel_decay_raw,
    token_decay_boost,
    output_projection_weight,
    expert_norm_gain,
    routes,
    expert_pair_weight,
    gate_weight,
    up_weight,
    down_weight,
):
    tokens_here, channels = recurrent_input.shape
    taps = filter_weight.shape[0]
    rim = shifted(recurrent_input[tokens_here - taps + 1 :], "sp", 1)
    extended = jnp.concatenate([rim, recurrent_input], axis=0).astype(jnp.float32)
    mixed_in = extended[0:tokens_here] * filter_weight[0]
    for offset in range(1, taps):
        mixed_in = mixed_in + extended[offset : offset + tokens_here] * filter_weight[offset]
    smoothed = mixed_in.astype(jnp.bfloat16)
    grouped = smoothed.reshape(
        tokens_here, recurrence_gate_matrix.shape[0], recurrence_gate_matrix.shape[1]
    )
    recurrence_gate = jax.nn.sigmoid(
        jnp.einsum(
            "tni,nij->tnj", grouped, recurrence_gate_matrix, preferred_element_type=jnp.float32
        ).reshape(tokens_here, channels)
    )
    input_gate = jax.nn.sigmoid(
        jnp.einsum(
            "tni,nij->tnj", grouped, input_gate_matrix, preferred_element_type=jnp.float32
        ).reshape(tokens_here, channels)
    )
    decay_logarithm = (
        -RECURRENT_SCALE * recurrence_gate * jax.nn.softplus(-channel_decay_raw) + token_decay_boost
    )
    decay = jnp.exp(decay_logarithm)
    drive = jnp.sqrt(-jnp.expm1(2.0 * decay_logarithm)) * (
        input_gate * smoothed.astype(jnp.float32)
    )
    running, local_state = lax.associative_scan(chain_step, (decay, drive), axis=0)
    identity = (jnp.ones((channels,), jnp.float32), jnp.zeros((channels,), jnp.float32))
    carried = carried_in((running[-1], local_state[-1]), "sp", chain_step, identity)
    state = local_state + running * carried[1][None, :]
    branch = (jax.nn.gelu(recurrent_out_gate.astype(jnp.float32)) * state).astype(jnp.bfloat16)
    tp_size = lax.axis_size("tp")
    rows_dev = tokens_here // tp_size
    projected = sum_at_owner(
        jnp.dot(branch, output_projection_weight, preferred_element_type=jnp.float32).astype(
            jnp.bfloat16
        ),
        "tp",
        0,
    )
    stream = (resid.astype(jnp.float32) + projected).astype(jnp.bfloat16)
    stream_wide = stream.astype(jnp.float32)
    normed = (
        stream_wide
        * lax.rsqrt(jnp.mean(stream_wide * stream_wide, axis=1, keepdims=True) + EPSILON)
        * expert_norm_gain
    ).astype(jnp.bfloat16)
    model_width = normed.shape[1]
    experts = lax.axis_size("sp")
    capacity = max(2, 3 * rows_dev // experts)
    own_routes = lax.dynamic_slice_in_dim(routes, lax.axis_index("tp") * rows_dev, rows_dev, 0)
    own_flat, own_rank = slot_numbers(own_routes, experts)
    own_slots = own_flat * capacity + own_rank
    row_of = jnp.arange(2 * rows_dev, dtype=jnp.int32) // 2
    outgoing = fill_slots(normed, own_slots, row_of, experts * capacity).reshape(
        experts, capacity, model_width
    )
    arrived = lax.all_to_all(outgoing, "sp", split_axis=0, concat_axis=0, tiled=True)

    def hidden_piece(piece, start):
        flat_rows = piece.reshape(piece.shape[0] * piece.shape[1], model_width)
        return expert_hidden(flat_rows, gate_weight, up_weight).reshape(
            piece.shape[0], piece.shape[1], -1
        )

    active = piecewise(
        arrived.reshape(1, experts * capacity, model_width), "tp", 0, hidden_piece, 0
    )
    result = expert_down(active.reshape(-1, active.shape[2]), down_weight)
    joined = lax.all_to_all(
        result.reshape(tp_size, experts * capacity, -1),
        "tp",
        split_axis=0,
        concat_axis=2,
        tiled=True,
    )
    returned = lax.all_to_all(
        joined.reshape(experts, capacity, model_width),
        "sp",
        split_axis=0,
        concat_axis=0,
        tiled=True,
    )
    picked = (
        returned.reshape(experts * capacity, model_width)[own_slots]
        .astype(jnp.float32)
        .reshape(rows_dev, 2, model_width)
    )
    blended = jnp.sum(picked * expert_pair_weight[:, :, None], axis=1)
    return (stream_wide + blended).astype(jnp.bfloat16)


def solution(mesh):
    placed = (
        P(("sp", "tp"), None),
        P("sp", "tp"),
        P("sp", "tp"),
        P(None, "tp"),
        P("tp", None, None),
        P("tp", None, None),
        P("tp"),
        P("sp", "tp"),
        P("tp", None),
        P(),
        P("sp", None),
        P(("sp", "tp"), None),
        P("sp", None, "tp"),
        P("sp", None, "tp"),
        P("sp", None, "tp"),
    )
    return jax.shard_map(
        body, mesh=mesh, in_specs=placed, out_specs=P(("sp", "tp"), None), check_vma=False
    )
```

profile of v0, /device:TPU:1, one launch (start us, length us, event | category | flops | bytes accessed | tf_op | source)
XLA Modules:
  0.0 395.7 jit_solution(9061123407506774359)
XLA Ops:
  7.4 3.9 collective-permute-start
  13.9 1.1 copy.87
  17.5 1.0 fusion.15
  19.0 4.5 %slice.371 = f32[256,128]{0,1:T(8,128)S(1)} slice(f32[512,128]{0,1:T(8,128)S(1)} %get-tuple-element.9), slice={[0:511:2], [0:128:1]} | slice | bytes 262144 | tf_op jit(solution)/shard_map/slice | solution.py:164
  23.5 4.5 %slice.372 = f32[256,128]{0,1:T(8,128)S(1)} slice(f32[512,128]{0,1:T(8,128)S(1)} %get-tuple-element.9), slice={[1:512:2], [0:128:1]} | slice | bytes 262144 | tf_op jit(solution)/shard_map/slice | solution.py:164
  27.9 4.5 %slice.370 = f32[256,128]{0,1:T(8,128)S(1)} slice(f32[512,128]{0,1:T(8,128)S(1)} %get-tuple-element.10), slice={[1:512:2], [0:128:1]} | slice | bytes 262144 | tf_op jit(solution)/shard_map/slice | solution.py:164
  32.4 5.0 %slice.374 = f32[256,128]{0,1:T(8,128)S(1)} slice(f32[512,128]{0,1:T(8,128)S(1)} %get-tuple-element.10), slice={[0:511:2], [0:128:1]} | slice | bytes 262144 | tf_op jit(solution)/shard_map/slice | solution.py:164
  37.5 2.2 slice.377
  39.7 2.2 slice.378
  41.9 2.2 slice.376
  44.1 2.2 slice.380
  46.3 1.1 slice.383
  47.5 1.2 slice.384
  48.6 1.2 slice.382
  49.8 1.1 slice.386
  60.3 1.1 slice.381
  61.5 1.1 slice.430
  62.6 2.2 slice.375
  64.8 2.2 slice.432
  67.1 4.5 %slice.369 = f32[255,128]{0,1:T(8,128)S(1)} slice(f32[512,128]{0,1:T(8,128)S(1)} %get-tuple-element.10), slice={[2:512:2], [0:128:1]} | slice | bytes 261120 | tf_op jit(solution)/shard_map/slice | solution.py:164
  71.5 4.9 %slice.434 = f32[255,128]{0,1:T(8,128)S(1)} slice(f32[512,128]{0,1:T(8,128)S(1)} %get-tuple-element.9), slice={[2:512:2], [0:128:1]} | slice | bytes 261120 | tf_op jit(solution)/shard_map/slice | solution.py:164
  84.9 1.1 pad.140
  86.0 1.1 pad.141
  87.2 1.1 pad.123
  88.4 1.1 pad.122
  89.7 2.2 pad.142
  91.9 2.2 pad.143
  94.1 4.5 %pad.145 = f32[512,128]{0,1:T(8,128)S(1)} pad(f32[256,128]{0,1:T(8,128)S(1)} %add.346, f32[]{:T(128)} %constant.25.clone.1), padding=1_0_1x0_0_0 | pad | bytes 393220 | tf_op jit(solution)/shard_map/pad | solution.py:164
  98.7 2.2 pad.124
  100.9 2.2 pad.125
  103.3 4.4 %pad.144 = f32[512,128]{0,1:T(8,128)S(1)} pad(f32[256,128]{0,1:T(8,128)S(1)} %pad_maximum_fusion.1, f32[]{:T(128)} %constant.25.clone.1), padding=0_1_1x0_0_0 | pad | bytes 393220 | tf_op jit(solution)/shard_map/pad | solution.py:164
  107.9 4.6 %pad.127 = f32[512,128]{0,1:T(8,128)S(1)} pad(f32[256,128]{0,1:T(8,128)S(1)} %add.336, f32[]{:T(128)} %constant.25.clone.1), padding=1_0_1x0_0_0 | pad | bytes 393220 | tf_op jit(solution)/shard_map/pad | solution.py:164
  112.6 4.4 %pad.126 = f32[512,128]{0,1:T(8,128)S(1)} pad(f32[256,128]{0,1:T(8,128)S(1)} %pad_maximum_fusion, f32[]{:T(128)} %constant.25.clone.1), padding=0_1_1x0_0_0 | pad | bytes 393220 | tf_op jit(solution)/shard_map/pad | solution.py:164
  117.8 12.6 %all-to-all-start = ((f32[32,2,128]{2,1,0:T(2,128)}), f32[32,2,128]{2,1,0:T(2,128)S(1)}, u32[]{:S(2)}, u32[]{:S(2)}) async-start(f32[32,2,128]{2,1,0:T(2,128)} %broadcast_in_dim.64), calls=%async_computation | async-start | bytes 65536 | tf_op jit(solution)/shard_map/all_to_all | solution.py:18
  130.4 8.7 %all-to-all-done = f32[32,2,128]{2,1,0:T(2,128)S(1)} async-done(((f32[32,2,128]{2,1,0:T(2,128)}), f32[32,2,128]{2,1,0:T(2,128)S(1)}, u32[]{:S(2)}, u32[]{:S(2)}) %all-to-all-start) | async-done | bytes 32800 | tf_op jit(solution)/shard_map/all_to_all | solution.py:18
  139.5 2.2 convolution_convert_fusion
  141.7 9.5 %all-to-all-start.1 = ((bf16[16,32,2048]{2,1,0:T(8,128)(2,1)}), bf16[16,32,2048]{2,1,0:T(8,128)(2,1)S(1)}, u32[]{:S(2)}, u32[]{:S(2)}) async-start(bf16[16,32,2048]{2,1,0:T(8,128)(2,1)} %bitcast.12), calls=%async_computation.1 | async-start | bytes 4194304 | tf_op jit(solution)/shard_map/all_to_all | solution.py:67
  152.9 47.3 %all-to-all-done.1 = bf16[16,32,2048]{2,1,0:T(8,128)(2,1)S(1)} async-done(((bf16[16,32,2048]{2,1,0:T(8,128)(2,1)}), bf16[16,32,2048]{2,1,0:T(8,128)(2,1)S(1)}, u32[]{:S(2)}, u32[]{:S(2)}) %all-to-all-start.1) | async-done | bytes 2097184 | tf_op jit(solution)/shard_map/all_to_all | solution.py:67
  202.3 19.6 %all_to_all.35 = bf16[32,3,2048]{2,1,0:T(4,128)(2,1)S(1)} all-to-all(bf16[32,3,2048]{2,1,0:T(4,128)(2,1)S(1)} %broadcast_select_fusion), channel_id=1, replica_groups=mesh['sp'=32,'tp'=16] {'sp'}, dimensions={0} | all-to-all | bytes 786432 | tf_op jit(solution)/shard_map/all_to_all | solution.py:195
  221.9 1.1 all_gather_reshape.3
  223.3 43.7 %all-gather.3.cloned.1.call-done = bf16[16,1,96,2048]{3,2,1,0:T(8,128)(2,1)} async-done(((bf16[1,1,96,2048]{3,2,1,0:T(8,128)(2,1)}), bf16[16,1,96,2048]{3,2,1,0:T(8,128)(2,1)}) %all-gather.3.cloned.1.call-update) | async-done | bytes 6291472 | tf_op jit(solution)/shard_map/all_gather | solution.py:81
  267.0 4.7 %fusion.2 = f32[16,96,128]{2,1,0:T(8,128)S(1)} fusion(bf16[16,1,96,2048]{3,2,1,0:T(8,128)(2,1)} %all-gather.3.cloned.1.call-done, bf16[1,2048,128]{2,1,0:T(8,128)(2,1)S(1)} %copy-done.5), kind=kOutput, calls=%fused_computation.4 | convolution fusion | flops 805306368 | bytes 7602176 | tf_op jit(solution)/shard_map/vmap()/dot_general | solution.py:105
  271.7 2.6 fusion.7
  274.4 58.5 %all-gather.5.cloned.1.call-done = bf16[1536,2048]{1,0:T(8,128)(2,1)} async-done(((bf16[1536,128]{1,0:T(8,128)(2,1)}), bf16[1536,2048]{1,0:T(8,128)(2,1)}) %all-gather.5.cloned.1.call-update) | async-done | bytes 6291472 | tf_op jit(solution)/shard_map/all_gather | solution.py:113
  332.9 4.6 %convolution_convert_fusion.1 = bf16[1536,128]{1,0:T(8,128)(2,1)S(1)} fusion(bf16[1536,2048]{1,0:T(8,128)(2,1)} %all-gather.5.cloned.1.call-done, bf16[1,2048,128]{2,1,0:T(8,128)(2,1)S(1)} %copy-done.7), kind=kOutput, calls=%fused_computation.8 | convolution fusion | flops 805502976 | bytes 7208960 | tf_op jit(solution)/shard_map/dot_general | solution.py:112
  337.5 19.4 %all_to_all.36 = bf16[16,96,128]{2,1,0:T(8,128)(2,1)S(1)} all-to-all(bf16[16,96,128]{2,1,0:T(8,128)(2,1)S(1)} %bitcast.97), channel_id=1, replica_groups=mesh['sp'=32,'tp'=16] {'tp'}, dimensions={0} | all-to-all | bytes 786432 | tf_op jit(solution)/shard_map/all_to_all | solution.py:207
  357.9 9.9 %all-to-all-start.4 = ((bf16[32,3,2048]{2,1,0:T(4,128)(2,1)}), bf16[32,3,2048]{2,1,0:T(4,128)(2,1)S(1)}, u32[]{:S(2)}, u32[]{:S(2)}) async-start(bf16[32,3,2048]{2,1,0:T(4,128)(2,1)} %reshape.148), calls=%async_computation.4 | async-start | bytes 1048576 | tf_op jit(solution)/shard_map/all_to_all | solution.py:214
  368.2 17.4 %all-to-all-done.4 = bf16[32,3,2048]{2,1,0:T(4,128)(2,1)S(1)} async-done(((bf16[32,3,2048]{2,1,0:T(4,128)(2,1)}), bf16[32,3,2048]{2,1,0:T(4,128)(2,1)S(1)}, u32[]{:S(2)}, u32[]{:S(2)}) %all-to-all-start.4) | async-done | bytes 393248 | tf_op jit(solution)/shard_map/all_to_all | solution.py:214
  (207 shorter events, 33.9 us)
Async XLA Ops:
  6.5 133.0 %copy-start = (bf16[128,2048]{1,0:T(8,128)(2,1)S(1)}, bf16[128,2048]{1,0:T(8,128)(2,1)}, u32[]{:S(2)}) copy-start(bf16[128,2048]{1,0:T(8,128)(2,1)} %param.23) | copy-start | bytes 1572868
  7.4 8.6 %collective-permute-start = (bf16[3,128]{0,1:T(8,128)(2,1)S(1)}, bf16[3,128]{0,1:T(8,128)(2,1)S(1)}, u32[]{:S(2)}, u32[]{:S(2)}) collective-permute-start(bf16[3,128]{0,1:T(8,128)(2,1)S(1)} %copy.84), channel_id=1, source_target_pairs={{0,16},{16,32},{32,48},{48,64},{64,80},{80,96},{96,112},{112,128},... | collective-permute-start | bytes 2312 | tf_op jit(solution)/shard_map/ppermute | solution.py:13
  107.8 92.8 %copy-start.1 = (bf16[32,2048]{1,0:T(8,128)(2,1)S(1)}, bf16[32,2048]{1,0:T(8,128)(2,1)}, u32[]{:S(2)}) copy-start(bf16[32,2048]{1,0:T(8,128)(2,1)} %param.15) | copy-start | bytes 393220
  112.4 88.3 %copy-start.2 = (f32[2048]{0:T(1024)S(1)}, f32[2048]{0:T(1024)}, u32[]{:S(2)}) copy-start(f32[2048]{0:T(1024)} %param.24) | copy-start | bytes 24580
  117.8 21.3 %all-to-all-start = ((f32[32,2,128]{2,1,0:T(2,128)}), f32[32,2,128]{2,1,0:T(2,128)S(1)}, u32[]{:S(2)}, u32[]{:S(2)}) async-start(f32[32,2,128]{2,1,0:T(2,128)} %broadcast_in_dim.64), calls=%async_computation | async-start | bytes 65536 | tf_op jit(solution)/shard_map/all_to_all | solution.py:18
  141.7 58.5 %all-to-all-start.1 = ((bf16[16,32,2048]{2,1,0:T(8,128)(2,1)}), bf16[16,32,2048]{2,1,0:T(8,128)(2,1)S(1)}, u32[]{:S(2)}, u32[]{:S(2)}) async-start(bf16[16,32,2048]{2,1,0:T(8,128)(2,1)} %bitcast.12), calls=%async_computation.1 | async-start | bytes 4194304 | tf_op jit(solution)/shard_map/all_to_all | solution.py:67
  151.2 115.8 %copy-start.5 = (bf16[1,2048,128]{2,1,0:T(8,128)(2,1)S(1)}, bf16[1,2048,128]{2,1,0:T(8,128)(2,1)}, u32[]{:S(2)}) copy-start(bf16[1,2048,128]{2,1,0:T(8,128)(2,1)} %param.27) | copy-start | bytes 1572868
  151.2 115.8 %all-gather.3.cloned.1.call-start = ((), (), s32[]{:S(2)}) async-start(), calls=%async_computation.5 | async-start | bytes 6684672 | tf_op jit(solution)/shard_map/all_gather | solution.py:81
  223.0 48.8 %copy-start.6 = (bf16[1,2048,128]{2,1,0:T(8,128)(2,1)S(1)}, bf16[1,2048,128]{2,1,0:T(8,128)(2,1)}, u32[]{:S(2)}) copy-start(bf16[1,2048,128]{2,1,0:T(8,128)(2,1)} %param.28) | copy-start | bytes 1572868
  223.0 109.9 %all-gather.5.cloned.1.call-start = ((), (), s32[]{:S(2)}) async-start(), calls=%async_computation.6 | async-start | bytes 6684672 | tf_op jit(solution)/shard_map/all_gather | solution.py:113
  267.0 4.8 %copy-start.4 = (bf16[16,1,96,2048]{3,2,1,0:T(8,128)(2,1)S(1)}, bf16[16,1,96,2048]{3,2,1,0:T(8,128)(2,1)}, u32[]{:S(2)}) copy-start(bf16[16,1,96,2048]{3,2,1,0:T(8,128)(2,1)} %all-gather.3.cloned.1.call-done) | copy-start | bytes 18874372
  271.7 61.1 %copy-start.7 = (bf16[1,2048,128]{2,1,0:T(8,128)(2,1)S(1)}, bf16[1,2048,128]{2,1,0:T(8,128)(2,1)}, u32[]{:S(2)}) copy-start(bf16[1,2048,128]{2,1,0:T(8,128)(2,1)} %param.29) | copy-start | bytes 1572868
  274.3 93.7 %copy-start.3 = (f32[32,2]{0,1:T(2,128)S(1)}, f32[32,2]{0,1:T(2,128)}, u32[]{:S(2)}) copy-start(f32[32,2]{0,1:T(2,128)} %param.26) | copy-start | bytes 772
  357.9 27.6 %all-to-all-start.4 = ((bf16[32,3,2048]{2,1,0:T(4,128)(2,1)}), bf16[32,3,2048]{2,1,0:T(4,128)(2,1)S(1)}, u32[]{:S(2)}, u32[]{:S(2)}) async-start(bf16[32,3,2048]{2,1,0:T(4,128)(2,1)} %reshape.148), calls=%async_computation.4 | async-start | bytes 1048576 | tf_op jit(solution)/shard_map/all_to_all | solution.py:214
Sparse Core Ops, SparseCore 0:
  223.1 43.8 all-gather.2
  274.5 58.3 all-gather.4
where the time goes:
time: 403 us; the launch traced here: 396 us
  waiting for transfers between devices  176 us (44%)
  local copies, waits for them, and re-layouts  105 us (26%)
  blocking collectives  39 us (10%)
  starting transfers between devices  36.2 us (9%)
  matrix products  16.1 us (4%)
  between operations  15.1 us (4%)
  other arithmetic  8.3 us (2%)
    all_gather x1, waiting for transfers between devices, expert_down(): lax.all_gather(active, 'tp', axis=1, tiled=True)  58.5 us
    slice x50, local copies, waits for them, and re-layouts, body(): lax.associative_scan(chain_step, (decay, drive), axis=0)  56 us
    all_to_all x1, waiting for transfers between devices, sum_at_owner(): lax.all_to_all(pieces, axis, split_axis=0, concat_axis=0, tiled=True)  47.3 us
    all_gather x1, waiting for transfers between devices, piecewise(): blocks = [lax.all_gather(slab, axis) for slab in pieces]  43.7 us
    pad x32, local copies, waits for them, and re-layouts, body(): lax.associative_scan(chain_step, (decay, drive), axis=0)  36.4 us
    all_to_all x1, blocking collectives, body(): lax.all_to_all(outgoing, 'sp', split_axis=0, concat_axis=0, tiled=True)  19.6 us
    all_to_all x1, blocking collectives, body(): lax.all_to_all(result.reshape(tp_size, experts * capacity, -1), 'tp', spl...  19.4 us
    all_to_all x1, waiting for transfers between devices, body(): lax.all_to_all(joined.reshape(experts, capacity, model_width), 'sp', spli...  17.4 us
  transfers between devices with their start and end apart: 6, of which 5 were waited for; matrix products, arithmetic and copies ran while one was open for 2% of the time, Pallas kernels for 0%

commit v1 on v0

--- a/solution.py
+++ b/solution.py
@@ -109,11 +109,17 @@
 
 def expert_down(active, down_weight):
     columns = down_weight[0]
-    return jnp.dot(
-        lax.all_gather(active, "tp", axis=1, tiled=True),
-        columns,
-        preferred_element_type=jnp.float32,
-    ).astype(jnp.bfloat16)
+
+    def body_move(x0):
+        x_new = lax.axis_size("tp")
+        arr_next = jnp.stack([x0] * x_new, 0)
+        next_value = lax.all_to_all(arr_next, "tp", 0, 0)
+        raw_out = jnp.concatenate(next_value, 1)
+        return raw_out
+
+    return jnp.dot(body_move(active), columns, preferred_element_type=jnp.float32).astype(
+        jnp.bfloat16
+    )
 
 
 def body(

time: 403 us -> 485 us (1.20)
  blocking collectives: 39 us -> 182 us
  waiting for transfers between devices: 176 us -> 117 us
    all_to_all x0 -> x1, blocking collectives: none -> 145 us  [body_move(): next_value = lax.all_to_all(arr_next, 'tp', 0, 0)]
    all_gather x1 -> x0, waiting for transfers between devices: 58.5 us -> none  [expert_down(): lax.all_gather(active, 'tp', axis=1, tiled=True)]
  transfers between devices with their start and end apart: 6 -> 5, of which waited for: 5 -> 4; matrix products, arithmetic and copies ran while one was open for 2% -> 1% of each run, Pallas kernels for 0% -> 0%
where the time goes in v1:
time: 485 us; the launch traced here: 478 us
  blocking collectives  182 us (38%)
  waiting for transfers between devices  117 us (24%)
  local copies, waits for them, and re-layouts  106 us (22%)
  starting transfers between devices  35.9 us (7%)
  between operations  15.1 us (3%)
  matrix products  12.6 us (3%)
  other arithmetic  8.3 us (2%)
    all_to_all x1, blocking collectives, body_move(): next_value = lax.all_to_all(arr_next, 'tp', 0, 0)  145 us
    slice x50, local copies, waits for them, and re-layouts, body(): lax.associative_scan(chain_step, (decay, drive), axis=0)  56 us
    all_to_all x1, waiting for transfers between devices, sum_at_owner(): lax.all_to_all(pieces, axis, split_axis=0, concat_axis=0, tiled=True)  47.3 us
    all_gather x1, waiting for transfers between devices, piecewise(): blocks = [lax.all_gather(slab, axis) for slab in pieces]  44 us
    pad x32, local copies, waits for them, and re-layouts, body(): lax.associative_scan(chain_step, (decay, drive), axis=0)  36.4 us
    all_to_all x1, blocking collectives, body(): lax.all_to_all(outgoing, 'sp', split_axis=0, concat_axis=0, tiled=True)  19.9 us
    all_to_all x1, waiting for transfers between devices, body(): lax.all_to_all(joined.reshape(experts, capacity, model_width), 'sp', spli...  17.4 us
    all_to_all x1, blocking collectives, body(): lax.all_to_all(result.reshape(tp_size, experts * capacity, -1), 'tp', spl...  17.3 us
  transfers between devices with their start and end apart: 5, of which 4 were waited for; matrix products, arithmetic and copies ran while one was open for 1% of the time, Pallas kernels for 0%

profile of v1, /device:TPU:1, one launch (start us, length us, event | category | flops | bytes accessed | tf_op | source)
XLA Modules:
  0.0 477.9 jit_solution(17198584147014565074)
XLA Ops:
  7.4 3.9 collective-permute-start
  13.9 1.1 copy.89
  17.5 1.0 fusion.15
  19.0 4.5 slice.371
  23.5 4.5 slice.372
  27.9 4.5 slice.370
  32.4 5.0 %slice.374 = f32[256,128]{0,1:T(8,128)S(1)} slice(f32[512,128]{0,1:T(8,128)S(1)} %get-tuple-element.10), slice={[0:511:2], [0:128:1]} | slice | bytes 262144 | tf_op jit(solution)/shard_map/slice | solution.py:170
  37.5 2.2 slice.377
  39.7 2.2 slice.378
  41.9 2.2 slice.376
  44.1 2.2 slice.380
  46.3 1.1 slice.383
  47.5 1.2 slice.384
  48.6 1.2 slice.382
  49.8 1.1 slice.386
  60.3 1.1 slice.381
  61.5 1.1 slice.430
  62.6 2.2 slice.375
  64.8 2.2 slice.432
  67.1 4.5 slice.369
  71.5 4.9 %slice.434 = f32[255,128]{0,1:T(8,128)S(1)} slice(f32[512,128]{0,1:T(8,128)S(1)} %get-tuple-element.9), slice={[2:512:2], [0:128:1]} | slice | bytes 261120 | tf_op jit(solution)/shard_map/slice | solution.py:170
  84.9 1.1 pad.140
  86.0 1.1 pad.141
  87.2 1.1 pad.123
  88.4 1.1 pad.122
  89.7 2.2 pad.142
  91.9 2.2 pad.143
  94.1 4.5 pad.145
  98.7 2.2 pad.124
  100.9 2.2 pad.125
  103.3 4.4 pad.144
  107.9 4.6 pad.127
  112.6 4.4 pad.126
  117.8 12.6 %all-to-all-start = ((f32[32,2,128]{2,1,0:T(2,128)}), f32[32,2,128]{2,1,0:T(2,128)S(1)}, u32[]{:S(2)}, u32[]{:S(2)}) async-start(f32[32,2,128]{2,1,0:T(2,128)} %broadcast_in_dim.64), calls=%async_computation | async-start | bytes 65536 | tf_op jit(solution)/shard_map/all_to_all | solution.py:18
  130.4 8.7 %all-to-all-done = f32[32,2,128]{2,1,0:T(2,128)S(1)} async-done(((f32[32,2,128]{2,1,0:T(2,128)}), f32[32,2,128]{2,1,0:T(2,128)S(1)}, u32[]{:S(2)}, u32[]{:S(2)}) %all-to-all-start) | async-done | bytes 32800 | tf_op jit(solution)/shard_map/all_to_all | solution.py:18
  139.5 2.2 convolution_convert_fusion
  141.7 9.5 %all-to-all-start.1 = ((bf16[16,32,2048]{2,1,0:T(8,128)(2,1)}), bf16[16,32,2048]{2,1,0:T(8,128)(2,1)S(1)}, u32[]{:S(2)}, u32[]{:S(2)}) async-start(bf16[16,32,2048]{2,1,0:T(8,128)(2,1)} %bitcast.12), calls=%async_computation.1 | async-start | bytes 4194304 | tf_op jit(solution)/shard_map/all_to_all | solution.py:67
  152.9 47.3 %all-to-all-done.1 = bf16[16,32,2048]{2,1,0:T(8,128)(2,1)S(1)} async-done(((bf16[16,32,2048]{2,1,0:T(8,128)(2,1)}), bf16[16,32,2048]{2,1,0:T(8,128)(2,1)S(1)}, u32[]{:S(2)}, u32[]{:S(2)}) %all-to-all-start.1) | async-done | bytes 2097184 | tf_op jit(solution)/shard_map/all_to_all | solution.py:67
  202.3 19.9 %all_to_all.40 = bf16[32,3,2048]{2,1,0:T(4,128)(2,1)S(1)} all-to-all(bf16[32,3,2048]{2,1,0:T(4,128)(2,1)S(1)} %broadcast_select_fusion), channel_id=1, replica_groups=mesh['sp'=32,'tp'=16] {'sp'}, dimensions={0} | all-to-all | bytes 786432 | tf_op jit(solution)/shard_map/all_to_all | solution.py:201
  222.1 1.1 all_gather_reshape.3
  223.2 44.0 %all-gather.2.cloned.1.call-done = bf16[16,1,96,2048]{3,2,1,0:T(8,128)(2,1)} async-done(((bf16[1,1,96,2048]{3,2,1,0:T(8,128)(2,1)}), bf16[16,1,96,2048]{3,2,1,0:T(8,128)(2,1)}) %all-gather.2.cloned.1.call-update) | async-done | bytes 6291472 | tf_op jit(solution)/shard_map/all_gather | solution.py:81
  267.2 4.7 fusion.2
  272.0 1.8 fusion.7
  274.6 145.3 %all_to_all.41 = bf16[16,1536,128]{1,2,0:T(8,128)(2,1)S(1)} all-to-all(bf16[16,1536,128]{1,2,0:T(8,128)(2,1)S(1)} %stack.3), channel_id=1, replica_groups=mesh['sp'=32,'tp'=16] {'tp'}, dimensions={0} | all-to-all | bytes 12582912 | tf_op jit(solution)/shard_map/all_to_all | solution.py:116
  420.0 1.8 convolution_convert_fusion.1
  421.8 17.3 %all_to_all.42 = bf16[16,96,128]{2,1,0:T(8,128)(2,1)S(1)} all-to-all(bf16[16,96,128]{2,1,0:T(8,128)(2,1)S(1)} %bitcast.101), channel_id=1, replica_groups=mesh['sp'=32,'tp'=16] {'tp'}, dimensions={0} | all-to-all | bytes 786432 | tf_op jit(solution)/shard_map/all_to_all | solution.py:213
  440.2 9.9 %all-to-all-start.5 = ((bf16[32,3,2048]{2,1,0:T(4,128)(2,1)}), bf16[32,3,2048]{2,1,0:T(4,128)(2,1)S(1)}, u32[]{:S(2)}, u32[]{:S(2)}) async-start(bf16[32,3,2048]{2,1,0:T(4,128)(2,1)} %reshape.173), calls=%async_computation.5 | async-start | bytes 1048576 | tf_op jit(solution)/shard_map/all_to_all | solution.py:220
  450.4 17.4 %all-to-all-done.5 = bf16[32,3,2048]{2,1,0:T(4,128)(2,1)S(1)} async-done(((bf16[32,3,2048]{2,1,0:T(4,128)(2,1)}), bf16[32,3,2048]{2,1,0:T(4,128)(2,1)S(1)}, u32[]{:S(2)}, u32[]{:S(2)}) %all-to-all-start.5) | async-done | bytes 393248 | tf_op jit(solution)/shard_map/all_to_all | solution.py:220
  (207 shorter events, 34.3 us)
Async XLA Ops:
  6.5 133.0 %copy-start = (bf16[128,2048]{1,0:T(8,128)(2,1)S(1)}, bf16[128,2048]{1,0:T(8,128)(2,1)}, u32[]{:S(2)}) copy-start(bf16[128,2048]{1,0:T(8,128)(2,1)} %param.23) | copy-start | bytes 1572868
  7.4 8.6 %collective-permute-start = (bf16[3,128]{0,1:T(8,128)(2,1)S(1)}, bf16[3,128]{0,1:T(8,128)(2,1)S(1)}, u32[]{:S(2)}, u32[]{:S(2)}) collective-permute-start(bf16[3,128]{0,1:T(8,128)(2,1)S(1)} %copy.86), channel_id=1, source_target_pairs={{0,16},{16,32},{32,48},{48,64},{64,80},{80,96},{96,112},{112,128},... | collective-permute-start | bytes 2312 | tf_op jit(solution)/shard_map/ppermute | solution.py:13
  107.8 92.8 %copy-start.1 = (bf16[32,2048]{1,0:T(8,128)(2,1)S(1)}, bf16[32,2048]{1,0:T(8,128)(2,1)}, u32[]{:S(2)}) copy-start(bf16[32,2048]{1,0:T(8,128)(2,1)} %param.15) | copy-start | bytes 393220
  112.4 88.3 %copy-start.2 = (f32[2048]{0:T(1024)S(1)}, f32[2048]{0:T(1024)}, u32[]{:S(2)}) copy-start(f32[2048]{0:T(1024)} %param.24) | copy-start | bytes 24580
  117.8 21.3 %all-to-all-start = ((f32[32,2,128]{2,1,0:T(2,128)}), f32[32,2,128]{2,1,0:T(2,128)S(1)}, u32[]{:S(2)}, u32[]{:S(2)}) async-start(f32[32,2,128]{2,1,0:T(2,128)} %broadcast_in_dim.64), calls=%async_computation | async-start | bytes 65536 | tf_op jit(solution)/shard_map/all_to_all | solution.py:18
  141.7 58.5 %all-to-all-start.1 = ((bf16[16,32,2048]{2,1,0:T(8,128)(2,1)}), bf16[16,32,2048]{2,1,0:T(8,128)(2,1)S(1)}, u32[]{:S(2)}, u32[]{:S(2)}) async-start(bf16[16,32,2048]{2,1,0:T(8,128)(2,1)} %bitcast.12), calls=%async_computation.1 | async-start | bytes 4194304 | tf_op jit(solution)/shard_map/all_to_all | solution.py:67
  151.2 116.1 %copy-start.5 = (bf16[1,2048,128]{2,1,0:T(8,128)(2,1)S(1)}, bf16[1,2048,128]{2,1,0:T(8,128)(2,1)}, u32[]{:S(2)}) copy-start(bf16[1,2048,128]{2,1,0:T(8,128)(2,1)} %param.27) | copy-start | bytes 1572868
  151.2 116.0 %all-gather.2.cloned.1.call-start = ((), (), s32[]{:S(2)}) async-start(), calls=%async_computation.6 | async-start | bytes 6684672 | tf_op jit(solution)/shard_map/all_gather | solution.py:81
  223.2 48.8 %copy-start.6 = (bf16[1,2048,128]{2,1,0:T(8,128)(2,1)S(1)}, bf16[1,2048,128]{2,1,0:T(8,128)(2,1)}, u32[]{:S(2)}) copy-start(bf16[1,2048,128]{2,1,0:T(8,128)(2,1)} %param.28) | copy-start | bytes 1572868
  267.2 4.8 copy-start.4
  274.6 145.4 %copy-start.7 = (bf16[1,2048,128]{2,1,0:T(8,128)(2,1)S(1)}, bf16[1,2048,128]{2,1,0:T(8,128)(2,1)}, u32[]{:S(2)}) copy-start(bf16[1,2048,128]{2,1,0:T(8,128)(2,1)} %param.29) | copy-start | bytes 1572868
  420.0 30.3 %copy-start.3 = (f32[32,2]{0,1:T(2,128)S(1)}, f32[32,2]{0,1:T(2,128)}, u32[]{:S(2)}) copy-start(f32[32,2]{0,1:T(2,128)} %param.26) | copy-start | bytes 772
  440.2 27.6 %all-to-all-start.5 = ((bf16[32,3,2048]{2,1,0:T(4,128)(2,1)}), bf16[32,3,2048]{2,1,0:T(4,128)(2,1)S(1)}, u32[]{:S(2)}, u32[]{:S(2)}) async-start(bf16[32,3,2048]{2,1,0:T(4,128)(2,1)} %reshape.173), calls=%async_computation.5 | async-start | bytes 1048576 | tf_op jit(solution)/shard_map/all_to_all | solution.py:220
Sparse Core Ops, SparseCore 0:
  223.4 43.8 all-gather.1
